TPU v7x, 32 devices: a whole 2x2x4 slice. The times are simulated.
32 devices in a mesh: rep: 2 (over x), fs: 8 (over z, y), tp: 2 (over core).
Axes of the slice: x: 2, y: 2, z: 4, core: 2. Of those that a mesh axis runs over, the one named last changes fastest.
Arguments:
- inputs: bfloat16 [8192, 2048], P(('rep', 'fs')), may hold values from -6 to 6
- cotangent: bfloat16 [8192, 2048], P(('rep', 'fs')), may hold values from -6 to 6
- gate_weight: bfloat16 [2048, 4096], P('fs', 'tp'), may hold values from -0.125 to 0.125
- up_weight: bfloat16 [2048, 4096], P('fs', 'tp'), may hold values from -0.125 to 0.125
- down_weight: bfloat16 [2048, 4096], P('fs', 'tp'), may hold values from -0.09375 to 0.09375
Outputs:
- grad_input: bfloat16 [8192, 2048], P(('rep', 'fs'))
- grad_down: float32 [2048, 4096], P('fs', 'tp')
All inputs are finite; a program needn't handle non-finite values.
Results may differ from a plain program's by a relative error of at most 0.014.
Values may be sent and summed in bfloat16 or wider, within the bound.
A program may use at most 128 MiB of HBM per device.

v0:
```python
import math

import jax
import jax.numpy as jnp
from jax import lax
from jax.sharding import PartitionSpec as P


def on_device(inputs, cotangent, gate_weight, up_weight, down_weight):
    tok_rows = inputs.shape[0]
    contract = (((1,), (1,)), ((), ()))
    contract_tok = (((0,), (0,)), ((), ()))
    gate_full, up_full, down_full = (
        lax.all_gather(gate_weight, "fs", axis=0, tiled=True),
        lax.all_gather(up_weight, "fs", axis=0, tiled=True),
        lax.all_gather(down_weight, "fs", axis=0, tiled=True),
    )
    gate_val = jnp.dot(inputs, gate_full, preferred_element_type=jnp.float32)
    up_val = jnp.dot(inputs, up_full, preferred_element_type=jnp.float32)
    grad_hidden = jnp.dot(cotangent, down_full, preferred_element_type=jnp.float32)
    sigmoid_gate = jax.nn.sigmoid(gate_val)
    active = gate_val * sigmoid_gate
    hidden = (active * up_val).astype(jnp.bfloat16)
    grad_gate = (
        grad_hidden * up_val * sigmoid_gate * (1.0 + gate_val * (1.0 - sigmoid_gate))
    ).astype(jnp.bfloat16)
    grad_up = (grad_hidden * active).astype(jnp.bfloat16)
    partial_value = lax.dot_general(
        grad_gate, gate_full, contract, preferred_element_type=jnp.float32
    )
    partial_value = partial_value + lax.dot_general(
        grad_up, up_full, contract, preferred_element_type=jnp.float32
    )
    grad_input = lax.psum(partial_value.astype(jnp.bfloat16), "tp")
    fs_size = lax.axis_size("fs")
    rep_size = lax.axis_size("rep")
    grad_scale = 1.0 / math.sqrt(tok_rows * fs_size * rep_size)
    grad_shard = lax.psum_scatter(
        lax.dot_general(cotangent, hidden, contract_tok, preferred_element_type=jnp.float32),
        "fs",
        scatter_dimension=0,
        tiled=True,
    )
    grad_down = lax.psum(grad_shard, "rep")
    return (grad_input, grad_down * grad_scale)


def solution(mesh):
    placed = (
        P(("rep", "fs"), None),
        P(("rep", "fs"), None),
        P("fs", "tp"),
        P("fs", "tp"),
        P("fs", "tp"),
    )
    return jax.shard_map(
        on_device,
        mesh=mesh,
        in_specs=placed,
        out_specs=(P(("rep", "fs"), None), P("fs", "tp")),
        check_vma=False,
    )
```

profile of v0, /device:TPU:0, one launch (start us, length us, event | category | flops | bytes accessed | tf_op | source)
XLA Modules:
  0.0 767.5 jit_solution(9472974704245236516)
XLA Ops:
  7.2 0.0 copy-start
  7.2 0.0 all-gather.8.cloned.1.call-start
  7.2 0.7 all-gather.8.cloned.1.call-update
  7.9 0.0 all-gather.6.cloned.1.call-start
  8.0 0.7 all-gather.6.cloned.1.call-update
  8.7 0.0 all-gather.4.cloned.1.call-start
  8.7 0.7 all-gather.4.cloned.1.call-update
  9.4 0.0 reduce-scatter.2.cloned.1.call-start
  9.4 127.9 %all-gather.8.cloned.1.call-done = bf16[2048,2048]{1,0:T(8,128)(2,1)} async-done(((bf16[256,2048]{1,0:T(8,128)(2,1)}), bf16[2048,2048]{1,0:T(8,128)(2,1)}) %all-gather.8.cloned.1.call-update) | async-done | bytes 8388624 | tf_op jit(solution)/shard_map/all_gather | solution.py:14
  137.3 10.4 %fusion.9 = f32[512,2048]{1,0:T(8,128)} fusion(bf16[512,2048]{1,0:T(8,128)(2,1)} %param.5, bf16[2048,2048]{1,0:T(8,128)(2,1)} %all-gather.8.cloned.1.call-done), kind=kOutput, calls=%fused_computation.14 | convolution fusion | flops 4294967296 | bytes 14680064 | tf_op jit(solution)/shard_map/dot_general | solution.py:18
  147.8 114.4 %all-gather.6.cloned.1.call-done = bf16[2048,2048]{1,0:T(8,128)(2,1)} async-done(((bf16[256,2048]{1,0:T(8,128)(2,1)}), bf16[2048,2048]{1,0:T(8,128)(2,1)}) %all-gather.6.cloned.1.call-update) | async-done | bytes 8388624 | tf_op jit(solution)/shard_map/all_gather | solution.py:15
  262.2 0.0 copy-start.2
  262.2 7.7 %fusion.8 = f32[512,2048]{1,0:T(8,128)S(1)} fusion(bf16[512,2048]{1,0:T(8,128)(2,1)} %param.5, bf16[2048,2048]{1,0:T(8,128)(2,1)} %all-gather.6.cloned.1.call-done), kind=kOutput, calls=%fused_computation.13 | convolution fusion | flops 4294967296 | bytes 14680064 | tf_op jit(solution)/shard_map/dot_general | solution.py:19
  269.9 0.0 copy-start.4
  269.9 2.0 copy-done.4
  271.9 0.0 copy-done
  271.9 0.0 copy-done.2
  271.9 8.2 %convolution_bitcast_fusion = f32[2048,2048]{0,1:T(8,128)} fusion(bf16[512,2048]{1,0:T(8,128)(2,1)S(1)} %copy-done, f32[512,2048]{1,0:T(8,128)S(1)} %fusion.8, f32[512,2048]{1,0:T(8,128)S(1)} %copy-done.2), kind=kOutput, calls=%fused_computation | convolution fusion | flops 4301258752 | bytes 27262976 | tf_op jit(solution)/shard_map/dot_general | solution.py:39
  280.2 0.0 reduce-scatter.2.cloned.1.call-update
  280.2 0.0 all-reduce.5.cloned.1.call-start
  280.2 106.8 %all-gather.4.cloned.1.call-done = bf16[2048,2048]{1,0:T(8,128)(2,1)} async-done(((bf16[256,2048]{1,0:T(8,128)(2,1)}), bf16[2048,2048]{1,0:T(8,128)(2,1)}) %all-gather.4.cloned.1.call-update) | async-done | bytes 8388624 | tf_op jit(solution)/shard_map/all_gather | solution.py:16
  387.0 9.4 %fusion.7 = f32[512,2048]{1,0:T(8,128)} fusion(bf16[512,2048]{1,0:T(8,128)(2,1)S(1)} %copy-done, bf16[2048,2048]{1,0:T(8,128)(2,1)} %all-gather.4.cloned.1.call-done), kind=kOutput, calls=%fused_computation.12 | convolution fusion | flops 4294967296 | bytes 14680064 | tf_op jit(solution)/shard_map/dot_general | solution.py:20
  396.4 272.7 %reduce-scatter.2.cloned.1.call-done = f32[256,2048]{0,1:T(8,128)} async-done(((f32[2048,2048]{0,1:T(8,128)}), f32[256,2048]{0,1:T(8,128)}) %reduce-scatter.2.cloned.1.call-update) | async-done | bytes 2097168 | tf_op jit(solution)/shard_map/reduce_scatter | solution.py:38
  669.1 0.0 all-reduce.5.cloned.1.call-update
  669.1 0.2 all-reduce.3.cloned.1.call-start
  669.3 0.0 copy-start.3
  669.3 15.6 %fusion.1 = f32[512,2048]{1,0:T(8,128)} fusion(bf16[2048,2048]{1,0:T(8,128)(2,1)} %all-gather.8.cloned.1.call-done, f32[512,2048]{1,0:T(8,128)} %fusion.9, f32[512,2048]{1,0:T(8,128)} %fusion.7, f32[512,2048]{1,0:T(8,128)} %copy-done.4), kind=kOutput, calls=%fused_computation.7 | convolution fusion | flops 4305453056 | bytes 25165824 | tf_op jit(solution)/shard_map/dot_general | solution.py:28
  684.9 0.0 copy-done.3
  684.9 11.7 %add_convert_fusion = bf16[512,2048]{1,0:T(8,128)(2,1)} fusion(f32[512,2048]{1,0:T(8,128)} %fusion.1, bf16[2048,2048]{1,0:T(8,128)(2,1)} %all-gather.6.cloned.1.call-done, f32[512,2048]{1,0:T(8,128)} %fusion.7, f32[512,2048]{1,0:T(8,128)S(1)} %copy-done.3), kind=kOutput, calls=%fused_computation.2 | convolution fusion | flops 4303355904 | bytes 23068672 | tf_op jit(solution)/shard_map/dot_general | solution.py:31
  696.6 0.0 all-reduce.3.cloned.1.call-update
  696.7 36.7 %all-reduce.5.cloned.1.call-done = f32[256,2048]{0,1:T(8,128)} async-done(((f32[256,2048]{0,1:T(8,128)}), f32[256,2048]{0,1:T(8,128)}) %all-reduce.5.cloned.1.call-update) | async-done | bytes 2097168 | tf_op jit(solution)/shard_map/psum | solution.py:44
  733.3 0.0 copy-start.1
  733.3 3.3 broadcast_multiply_fusion
  736.6 2.9 copy.7
  739.5 18.0 %all-reduce.3.cloned.1.call-done = bf16[512,2048]{1,0:T(8,128)(2,1)} async-done(((bf16[512,2048]{1,0:T(8,128)(2,1)}), bf16[512,2048]{1,0:T(8,128)(2,1)}) %all-reduce.3.cloned.1.call-update) | async-done | bytes 2097168 | tf_op jit(solution)/shard_map/psum | solution.py:34
  757.5 3.2 copy.10
  760.6 0.0 copy-done.1
Async XLA Ops:
  7.2 264.8 %copy-start = (bf16[512,2048]{1,0:T(8,128)(2,1)S(1)}, bf16[512,2048]{1,0:T(8,128)(2,1)}, u32[]{:S(2)}) copy-start(bf16[512,2048]{1,0:T(8,128)(2,1)} %param.6) | copy-start | bytes 6291460
  7.2 130.2 %all-gather.8.cloned.1.call-start = ((), (), s32[]{:S(2)}) async-start(), calls=%async_computation.3 | async-start | bytes 9437184 | tf_op jit(solution)/shard_map/all_gather | solution.py:14
  7.9 254.2 %all-gather.6.cloned.1.call-start = ((), (), s32[]{:S(2)}) async-start(), calls=%async_computation.2 | async-start | bytes 9437184 | tf_op jit(solution)/shard_map/all_gather | solution.py:15
  8.7 378.3 %all-gather.4.cloned.1.call-start = ((), (), s32[]{:S(2)}) async-start(), calls=%async_computation.1 | async-start | bytes 9437184 | tf_op jit(solution)/shard_map/all_gather | solution.py:16
  9.4 659.7 %reduce-scatter.2.cloned.1.call-start = ((), (), s32[]{:S(2)}) async-start(), calls=%async_computation.5 | async-start | bytes 18874368 | tf_op jit(solution)/shard_map/reduce_scatter | solution.py:38
  262.2 9.8 %copy-start.2 = (f32[512,2048]{1,0:T(8,128)S(1)}, f32[512,2048]{1,0:T(8,128)}, u32[]{:S(2)}) copy-start(f32[512,2048]{1,0:T(8,128)} %fusion.9) | copy-start | bytes 12582916
  269.9 2.1 copy-start.4
  280.2 453.2 %all-reduce.5.cloned.1.call-start = ((), (), s32[]{:S(2)}) async-start(), calls=%async_computation.6 | async-start | bytes 4194304 | tf_op jit(solution)/shard_map/psum | solution.py:44
  669.1 88.3 %all-reduce.3.cloned.1.call-start = ((), (), s32[]{:S(2)}) async-start(), calls=%async_computation.4 | async-start | bytes 4194304 | tf_op jit(solution)/shard_map/psum | solution.py:34
  669.3 15.6 %copy-start.3 = (f32[512,2048]{1,0:T(8,128)S(1)}, f32[512,2048]{1,0:T(8,128)}, u32[]{:S(2)}) copy-start(f32[512,2048]{1,0:T(8,128)} %fusion.9) | copy-start | bytes 12582916
  733.3 27.3 %copy-start.1 = (bf16[512,2048]{1,0:T(8,128)(2,1)S(1)}, bf16[512,2048]{1,0:T(8,128)(2,1)}, u32[]{:S(2)}) copy-start(bf16[512,2048]{1,0:T(8,128)(2,1)} %param.6) | copy-start | bytes 6291460
Sparse Core Ops, SparseCore 0:
  10.1 127.1 all-gather.7
  139.5 122.6 all-gather.5
  264.3 122.6 all-gather.3
  390.6 278.4 reduce-scatter.1
  671.2 62.0 all-reduce.4
  736.1 21.3 all-reduce.2
where the time goes:
time: 768 us; the launch traced here: 767 us
  waiting for transfers between devices  678 us (88%)
  matrix products  63.1 us (8%)
  between operations  14.1 us (2%)
  local copies, waits for them, and re-layouts  8.11 us (1%)
    reduce_scatter x1, waiting for transfers between devices, on_device(): lax.psum_scatter(lax.dot_general(cotangent, hidden, contract_tok, preferr...  273 us
    all_gather x1, waiting for transfers between devices, on_device(): lax.all_gather(gate_weight, 'fs', axis=0, tiled=True)  128 us
    all_gather x1, waiting for transfers between devices, on_device(): lax.all_gather(up_weight, 'fs', axis=0, tiled=True)  114 us
    all_gather x1, waiting for transfers between devices, on_device(): lax.all_gather(down_weight, 'fs', axis=0, tiled=True)  107 us
    psum x1, waiting for transfers between devices, on_device(): grad_down = lax.psum(grad_shard, 'rep')  36.7 us
    psum x1, waiting for transfers between devices, on_device(): grad_input = lax.psum(partial_value.astype(jnp.bfloat16), 'tp')  18 us
    dot_general x1, matrix products, on_device(): lax.dot_general(grad_gate, gate_full, contract, preferred_element_type=jn...  15.6 us
  transfers between devices with their start and end apart: 6, of which 6 were waited for; matrix products, arithmetic and copies ran while one was open for 9% of the time, Pallas kernels for 0%

commit v1 on v0

v1 whole, which is shorter than its diff:
```python
import functools
import math

import jax
import jax.numpy as jnp
from jax import lax
from jax.experimental import pallas as pl
from jax.experimental.pallas import tpu as pltpu
from jax.sharding import PartitionSpec as P

MESH = pl.DeviceIdType.MESH


def gather_kernel(
    line, parts, pieces, toks, cots, w_out, t_out, w_tmp, t_tmp,
    up_s, up_r, dn_s, dn_r, y_s, y_r, tok_s, tok_r, d2d_s, d2d_r, loc, loc2,
):
    r = lax.axis_index("rep")
    f = lax.axis_index("fs")
    t = lax.axis_index("tp")
    z, y = f // 2, f % 2
    rows = toks.shape[0]
    half = rows // 2
    wrows = pieces.shape[2]
    per = pieces.shape[1] // parts
    has_up, has_dn = z < line - 1, z > 0
    up = {"fs": (f + 2) % (2 * line)}
    dn = {"fs": (f + 2 * line - 2) % (2 * line)}
    ypart = {"fs": f + 1 - 2 * y}
    xpart = {"rep": 1 - r}
    core = t % 2
    cpart = {"tp": t + 1 - 2 * core}

    barrier = pltpu.get_barrier_semaphore()

    def greet(dev):
        pl.semaphore_signal(barrier, inc=1, device_id=dev, device_id_type=MESH)

    for dev in (ypart, xpart, cpart, up, dn):
        greet(dev)
    pl.semaphore_wait(barrier, 5)

    def remote(src, dst, s, q, dev):
        return pltpu.make_async_remote_copy(
            src_ref=src, dst_ref=dst, send_sem=s, recv_sem=q,
            device_id=dev, device_id_type=MESH,
        )

    def wblk(k, zz, yy):
        row = pl.multiple_of((2 * zz + yy) * wrows, wrows)
        return w_out.at[pl.ds(k * per, per), pl.ds(row, wrows), :]

    def own(k, yy):
        return pieces.at[yy, pl.ds(k * per, per)]

    def to_y(k):
        return remote(own(k, 1 - y), wblk(k, z, y), y_s.at[k], y_r.at[k], ypart)

    def from_y(k):
        return remote(own(k, 1 - y), wblk(k, z, 1 - y), y_s.at[k], y_r.at[k], ypart)

    def zcopy(up_dir, d, sub, k, zz):
        yy = y if sub == 0 else 1 - y
        src = own(k, y) if (d == 0 and sub == 0) else wblk(k, zz, yy)
        s, q, dev = (up_s, up_r, up) if up_dir else (dn_s, dn_r, dn)
        return remote(src, wblk(k, zz, yy), s.at[d, sub, k], q.at[d, sub, k], dev)

    def pred_send(up_dir, d):
        return (has_up & (z - d >= 0)) if up_dir else (has_dn & (z + d <= line - 1))

    def src_z(up_dir, d):
        return jnp.maximum(z - d, 0) if up_dir else jnp.minimum(z + d, line - 1)

    def send(up_dir, d, sub, k):
        @pl.when(pred_send(up_dir, d))
        def _():
            zcopy(up_dir, d, sub, k, src_z(up_dir, d)).start()

    def await_send(up_dir, d, sub, k):
        @pl.when(pred_send(up_dir, d))
        def _():
            zcopy(up_dir, d, sub, k, src_z(up_dir, d)).wait_send()

    def await_recv(up_dir, d, sub, k):
        ok = (z - d - 1 >= 0) if up_dir else (z + d + 1 <= line - 1)

        @pl.when(ok)
        def _():
            zcopy(up_dir, d, sub, k, src_z(up_dir, d + 1)).wait_recv()

    def tblk(j, rr, yy, c):
        row = pl.multiple_of((2 * rr + yy) * rows + c * half, half)
        return t_out.at[j, pl.ds(row, half), :]

    def mine(j):
        src = toks if j == 0 else cots
        return src.at[pl.ds(pl.multiple_of(core * half, half), half), :]

    def tcopy(i, landing):
        j = (0, 1, 0, 1, 0, 1)[i]
        dev = xpart if i in (0, 1, 5) else ypart
        if landing:
            rr = (1 - r, 1 - r, r, r, 1 - r, 1 - r)[i]
            yy = (y, y, 1 - y, 1 - y, 1 - y, 1 - y)[i]
            src = dst = tblk(j, rr, yy, core)
        else:
            rr = (r, r, r, r, 1 - r, r)[i]
            yy = (y, y, y, y, y, 1 - y)[i]
            dst = tblk(j, rr, yy, core)
            src = mine(j) if i < 4 else dst
        return remote(src, dst, tok_s.at[i], tok_r.at[i], dev)

    def dcopy(i, c):
        j = (0, 1, 0, 1, 0, 1)[i]
        rr = (1 - r, 1 - r, r, r, 1 - r, 1 - r)[i]
        yy = (y, y, 1 - y, 1 - y, 1 - y, 1 - y)[i]
        blk = tblk(j, rr, yy, c)
        return remote(blk, blk, d2d_s.at[i], d2d_r.at[i], cpart)

    loads = [
        pltpu.make_async_copy(pieces.at[y], w_tmp, loc.at[0]),
        pltpu.make_async_copy(toks, t_tmp.at[0], loc.at[1]),
        pltpu.make_async_copy(cots, t_tmp.at[1], loc.at[2]),
    ]
    trow = pl.multiple_of((2 * r + y) * rows, rows)
    wrow = pl.multiple_of(f * wrows, wrows)
    stores = [
        pltpu.make_async_copy(w_tmp, w_out.at[:, pl.ds(wrow, wrows), :], loc2.at[0]),
        pltpu.make_async_copy(t_tmp.at[0], t_out.at[0, pl.ds(trow, rows), :], loc2.at[1]),
        pltpu.make_async_copy(t_tmp.at[1], t_out.at[1, pl.ds(trow, rows), :], loc2.at[2]),
    ]

    for k in range(parts):
        to_y(k).start()
        send(True, 0, 0, k)
        send(False, 0, 0, k)
    for i in (0, 1, 3, 2):
        tcopy(i, False).start()
    for copy in loads:
        copy.start()
    for load, store in zip(loads, stores):
        load.wait()
        store.start()
    for k in range(parts):
        from_y(k).wait_recv()
        send(True, 0, 1, k)
        send(False, 0, 1, k)

    def event(i):
        tcopy(i, True).wait_recv()
        if i == 0:
            tcopy(4, False).start()
        if i == 3:
            tcopy(5, False).start()
        dcopy(i, core).start()

    events = [0, 3, 1, 2, 5, 4]
    for d in range(line - 1):
        for sub in range(2):
            if events:
                event(events.pop(0))
            for k in range(parts):
                for up_dir in (True, False):
                    await_recv(up_dir, d, sub, k)
                    if d + 1 < line - 1:
                        send(up_dir, d + 1, sub, k)
    for i in events:
        event(i)
    for i in range(6):
        dcopy(i, 1 - core).wait_recv()
        dcopy(i, core).wait_send()
        tcopy(i, False).wait_send()
    for k in range(parts):
        to_y(k).wait_send()
        for d in range(line - 1):
            for sub in range(2):
                await_send(True, d, sub, k)
                await_send(False, d, sub, k)
    for store in stores:
        store.wait()


def gather(pieces, toks, cots):
    line = lax.axis_size("fs") // 2
    kinds, wrows, width = pieces.shape[1:]
    parts = kinds if line <= 4 else 1
    dma = pltpu.SemaphoreType.DMA
    zsem = dma((line - 1, 2, parts))
    anyspec = pl.BlockSpec(memory_space=pl.ANY)
    return pl.pallas_call(
        functools.partial(gather_kernel, line, parts),
        out_shape=(
            jax.ShapeDtypeStruct((kinds, 2 * line * wrows, width), pieces.dtype),
            jax.ShapeDtypeStruct((2, 4 * toks.shape[0], toks.shape[1]), toks.dtype),
        ),
        in_specs=[anyspec] * 3,
        out_specs=(anyspec, anyspec),
        scratch_shapes=[
            pltpu.VMEM(pieces.shape[1:], pieces.dtype),
            pltpu.VMEM((2,) + toks.shape, toks.dtype),
            zsem, zsem, zsem, zsem,
            dma((parts,)), dma((parts,)),
            dma((6,)), dma((6,)), dma((6,)), dma((6,)),
            dma((3,)), dma((3,)),
        ],
        compiler_params=pltpu.CompilerParams(collective_id=0, has_side_effects=True),
        name="gather_all",
    )(pieces, toks, cots)


def on_device(inputs, cotangent, gate_weight, up_weight, down_weight):
    tok_rows = inputs.shape[0]
    fs_size = lax.axis_size("fs")
    rep_size = lax.axis_size("rep")
    contract = (((1,), (1,)), ((), ()))
    contract_tok = (((0,), (0,)), ((), ()))
    width = gate_weight.shape[1] // 4
    r = lax.axis_index("rep")
    y = lax.axis_index("fs") % 2

    def piece(side):
        return jnp.stack([
            lax.dynamic_slice_in_dim(weight, (2 * r + side) * width, width, 1)
            for weight in (gate_weight, up_weight, down_weight)
        ])

    weights, tokens = gather(jnp.stack([piece(0), piece(1)]), inputs, cotangent)
    gate_full, up_full, down_full = weights[0], weights[1], weights[2]
    gate_val = jnp.dot(tokens[0], gate_full, preferred_element_type=jnp.float32)
    up_val = jnp.dot(tokens[0], up_full, preferred_element_type=jnp.float32)
    grad_hidden = jnp.dot(tokens[1], down_full, preferred_element_type=jnp.float32)
    sigmoid_gate = jax.nn.sigmoid(gate_val)
    active = gate_val * sigmoid_gate
    hidden = (active * up_val).astype(jnp.bfloat16)
    grad_gate = (
        grad_hidden * up_val * sigmoid_gate * (1.0 + gate_val * (1.0 - sigmoid_gate))
    ).astype(jnp.bfloat16)
    grad_up = (grad_hidden * active).astype(jnp.bfloat16)
    grad_scale = 1.0 / math.sqrt(tok_rows * fs_size * rep_size)
    pairs = [[i, i + 1] for i in range(0, fs_size, 2)]
    lines = [list(range(i, fs_size, 2)) for i in range(2)]
    grad_part = lax.dot_general(
        tokens[1], hidden, contract_tok, preferred_element_type=jnp.float32
    )
    shard = lax.psum_scatter(
        grad_part.astype(jnp.bfloat16), "fs", scatter_dimension=0, tiled=True,
        axis_index_groups=lines,
    ).astype(jnp.float32) * grad_scale
    shard = lax.all_to_all(
        shard, "fs", split_axis=0, concat_axis=1, tiled=True, axis_index_groups=pairs
    )
    grad_down = lax.all_gather(shard, "rep", axis=1, tiled=True)
    part = lax.dot_general(
        grad_gate, gate_full, contract, preferred_element_type=jnp.float32
    )
    part = part + lax.dot_general(
        grad_up, up_full, contract, preferred_element_type=jnp.float32
    )
    part = lax.psum_scatter(
        part.astype(jnp.bfloat16), "rep", scatter_dimension=0, tiled=True
    )
    part = lax.psum_scatter(
        part, "fs", scatter_dimension=0, tiled=True, axis_index_groups=pairs
    )
    grad_input = lax.psum(part, "tp")
    return (grad_input, grad_down)


def solution(mesh):
    placed = (
        P(("rep", "fs"), None),
        P(("rep", "fs"), None),
        P("fs", "tp"),
        P("fs", "tp"),
        P("fs", "tp"),
    )
    return jax.shard_map(
        on_device,
        mesh=mesh,
        in_specs=placed,
        out_specs=(P(("rep", "fs"), None), P("fs", "tp")),
        check_vma=False,
    )
```

time: 768 us -> 449 us (0.58)
  waiting for transfers between devices: 678 us -> 228 us
  Pallas kernels: 0 us -> 108 us
  blocking collectives: 0 us -> 25.1 us
    all_gather x3 -> x1, waiting for transfers between devices: 349 us -> 33.7 us  [on_device(): grad_down = lax.all_gather(shard, 'rep', axis=1, tiled=True)]
    pallas_call x0 -> x1, Pallas kernels: none -> 108 us  [gather(): pl.pallas_call(functools.partial(gather_kernel, line, parts), out_shape=(...]
    reduce_scatter x1 -> x3, waiting for transfers between devices: 273 us -> 170 us  [the longest x1 87.6 us: on_device(): lax.psum_scatter(part.astype(jnp.bfloat16), 'rep', scatter_dimension=0, t...]
    psum x2 -> x1, waiting for transfers between devices: 54.6 us -> 23.5 us  [on_device(): grad_input = lax.psum(part, 'tp')]
    all_to_all x0 -> x1, blocking collectives: none -> 25.1 us  [on_device(): lax.all_to_all(shard, 'fs', split_axis=0, concat_axis=1, tiled=True, axis...]
  transfers between devices with their start and end apart: 6 -> 5, of which waited for: 6 -> 5; matrix products, arithmetic and copies ran while one was open for 9% -> 3% of each run, Pallas kernels for 0% -> 0%
where the time goes in v1:
time: 449 us
  waiting for transfers between devices  228 us (51%)
  Pallas kernels  108 us (24%)
  matrix products  59.3 us (13%)
  blocking collectives  25.1 us (6%)
  between operations  13.9 us (3%)
  local copies, waits for them, and re-layouts  12.8 us (3%)
    pallas_call x1, Pallas kernels, gather(): pl.pallas_call(functools.partial(gather_kernel, line, parts), out_shape=(...  108 us
    reduce_scatter x1, waiting for transfers between devices, on_device(): lax.psum_scatter(part.astype(jnp.bfloat16), 'rep', scatter_dimension=0, t...  87.6 us
    reduce_scatter x1, waiting for transfers between devices, on_device(): lax.psum_scatter(grad_part.astype(jnp.bfloat16), 'fs', scatter_dimension=...  46.5 us
    reduce_scatter x1, waiting for transfers between devices, on_device(): lax.psum_scatter(part, 'fs', scatter_dimension=0, tiled=True, axis_index_...  36.1 us
    all_gather x1, waiting for transfers between devices, on_device(): grad_down = lax.all_gather(shard, 'rep', axis=1, tiled=True)  33.7 us
    all_to_all x1, blocking collectives, on_device(): lax.all_to_all(shard, 'fs', split_axis=0, concat_axis=1, tiled=True, axis...  25.1 us
    psum x1, waiting for transfers between devices, on_device(): grad_input = lax.psum(part, 'tp')  23.5 us
    dot_general x1, matrix products, on_device(): lax.dot_general(grad_up, up_full, contract, preferred_element_type=jnp.fl...  16.8 us
  transfers between devices with their start and end apart: 5, of which 5 were waited for; matrix products, arithmetic and copies ran while one was open for 3% of the time, Pallas kernels for 0%

profile of v1, /device:TPU:0, one launch (start us, length us, event | category | flops | bytes accessed | tf_op | source)
XLA Modules:
  0.0 449.0 jit_solution(4309660888108420258)
XLA Ops:
  7.2 0.0 reduce-scatter.4.cloned.1.call-start
  7.2 1.1 dynamic-slice_bitcast_fusion.5
  8.3 1.3 dynamic-slice_bitcast_fusion.3
  9.6 0.1 maximum_bitcast_fusion
  9.7 0.1 maximum_bitcast_fusion.1
  9.8 1.3 pad_maximum_fusion.pieces
  11.0 107.5 %gather_all.1 = (bf16[3,2048,512]{2,1,0:T(8,128)(2,1)}, bf16[2,2048,2048]{2,1,0:T(8,128)(2,1)}) custom-call(bf16[2,3,256,512]{3,2,1,0:T(8,128)(2,1)} %pad_maximum_fusion.pieces, bf16[512,2048]{1,0:T(8,128)(2,1)} %toks.1, bf16[512,2048]{1,0:T(8,128)(2,1)} %cots.1), custom_call_target="tpu_custom_call" | custom-call | tf_op jit(solution)/shard_map/gather_all/pallas_call | solution.py:190
  118.6 0.0 copy-start.1
  118.6 0.0 copy-start.2
  118.6 7.7 %fusion = f32[2048,512]{1,0:T(8,128)S(1)} fusion(bf16[2,2048,2048]{2,1,0:T(8,128)(2,1)} %get-tuple-element.4, bf16[3,2048,512]{2,1,0:T(8,128)(2,1)} %get-tuple-element.5), kind=kOutput, calls=%fused_computation.1 | convolution fusion | flops 4294967296 | bytes 14680064 | tf_op jit(solution)/shard_map/dot_general | solution.py:229
  126.3 1.1 copy-done.1
  127.4 1.8 copy-done.2
  129.2 0.0 copy-start.3
  129.2 6.0 %fusion.2 = f32[2048,512]{1,0:T(8,128)} fusion(bf16[2,2048,2048]{2,1,0:T(8,128)(2,1)S(1)} %copy-done.1, bf16[3,2048,512]{2,1,0:T(8,128)(2,1)S(1)} %copy-done.2), kind=kOutput, calls=%fused_computation.3 | convolution fusion | flops 4294967296 | bytes 14680064 | tf_op jit(solution)/shard_map/dot_general | solution.py:230
  135.2 4.5 %fusion.6 = f32[2048,512]{1,0:T(8,128)S(1)} fusion(bf16[2,2048,2048]{2,1,0:T(8,128)(2,1)S(1)} %copy-done.1, bf16[3,2048,512]{2,1,0:T(8,128)(2,1)S(1)} %copy-done.2), kind=kOutput, calls=%fused_computation.7 | convolution fusion | flops 4294967296 | bytes 14680064 | tf_op jit(solution)/shard_map/dot_general | solution.py:231
  139.7 0.0 copy-done.3
  139.7 0.0 copy-start.4
  139.7 2.0 copy-done.4
  141.7 12.5 %fusion.16 = f32[2048,2048]{1,0:T(8,128)} fusion(f32[2048,512]{1,0:T(8,128)S(1)} %fusion, f32[2048,512]{1,0:T(8,128)S(1)} %fusion.6, f32[2048,512]{1,0:T(8,128)} %fusion.2, bf16[3,2048,512]{2,1,0:T(8,128)(2,1)S(1)} %copy-done.2), kind=kOutput, calls=%fused_computation.19 | convolution fusion | flops 4305453056 | bytes 31457280 | tf_op jit(solution)/shard_map/dot_general | solution.py:253
  154.2 16.8 %add_convert_fusion = bf16[2048,2048]{1,0:T(8,128)(2,1)} fusion(f32[2048,2048]{1,0:T(8,128)} %fusion.16, f32[2048,512]{1,0:T(8,128)} %copy-done.4, bf16[3,2048,512]{2,1,0:T(8,128)(2,1)} %get-tuple-element.5, f32[2048,512]{1,0:T(8,128)} %copy-done.3), kind=kOutput, calls=%fused_computation | convolution fusion | flops 4309647360 | bytes 35651584 | tf_op jit(solution)/shard_map/dot_general | solution.py:256
  171.0 0.0 reduce-scatter.4.cloned.1.call-update
  171.1 0.0 reduce-scatter.8.cloned.1.call-start
  171.1 11.8 %fusion.13 = bf16[2048,512]{1,0:T(8,128)(2,1)} fusion(bf16[2,2048,2048]{2,1,0:T(8,128)(2,1)} %get-tuple-element.4, f32[2048,512]{1,0:T(8,128)} %fusion.2, f32[2048,512]{1,0:T(8,128)} %copy-done.3), kind=kOutput, calls=%fused_computation.18 | convolution fusion | flops 4302307328 | bytes 18874368 | tf_op jit(solution)/shard_map/dot_general | solution.py:242
  182.9 0.0 reduce-scatter.8.cloned.1.call-update
  183.0 0.0 reduce-scatter.6.cloned.1.call-start
  183.0 87.6 %reduce-scatter.4.cloned.1.call-done = bf16[1024,2048]{1,0:T(8,128)(2,1)} async-done(((bf16[2048,2048]{1,0:T(8,128)(2,1)}), bf16[1024,2048]{1,0:T(8,128)(2,1)}) %reduce-scatter.4.cloned.1.call-update) | async-done | bytes 4194320 | tf_op jit(solution)/shard_map/reduce_scatter | solution.py:259
  270.6 0.0 reduce-scatter.6.cloned.1.call-update
  270.6 0.0 all-gather.2.cloned.1.call-start
  270.7 46.5 %reduce-scatter.8.cloned.1.call-done = bf16[512,512]{1,0:T(8,128)(2,1)} async-done(((bf16[2048,512]{1,0:T(8,128)(2,1)}), bf16[512,512]{1,0:T(8,128)(2,1)}) %reduce-scatter.8.cloned.1.call-update) | async-done | bytes 524304 | tf_op jit(solution)/shard_map/reduce_scatter | solution.py:245
  317.2 1.2 convert_multiply_fusion
  318.4 25.1 %all_to_all.19 = f32[2,256,512]{2,1,0:T(8,128)S(1)} all-to-all(f32[2,256,512]{2,1,0:T(8,128)S(1)} %bitcast.46), channel_id=1, replica_groups={{0,2},{4,6},{8,10},{12,14},{1,3},{5,7},{9,11},{13,15},{16,18},{20,22},{..., dimensions={0} | all-to-all | bytes 2097152 | tf_op jit(solution)/shard_map/all_to_all | solution.py:249
  343.5 1.1 copy.8
  344.6 0.0 all-gather.2.cloned.1.call-update
  344.6 0.0 all-reduce.2.cloned.1.call-start
  344.6 36.1 %reduce-scatter.6.cloned.1.call-done = bf16[512,2048]{1,0:T(8,128)(2,1)} async-done(((bf16[1024,2048]{1,0:T(8,128)(2,1)}), bf16[512,2048]{1,0:T(8,128)(2,1)}) %reduce-scatter.6.cloned.1.call-update) | async-done | bytes 2097168 | tf_op jit(solution)/shard_map/reduce_scatter | solution.py:262
  380.7 0.0 all-reduce.2.cloned.1.call-update
  380.7 33.7 %all-gather.2.cloned.1.call-done = f32[256,2048]{1,0:T(8,128)} async-done(((f32[256,1024]{1,0:T(8,128)}), f32[256,2048]{1,0:T(8,128)}) %all-gather.2.cloned.1.call-update) | async-done | bytes 2097168 | tf_op jit(solution)/shard_map/all_gather | solution.py:252
  414.5 0.0 copy-start
  414.5 23.5 %all-reduce.2.cloned.1.call-done = bf16[512,2048]{1,0:T(8,128)(2,1)} async-done(((bf16[512,2048]{1,0:T(8,128)(2,1)}), bf16[512,2048]{1,0:T(8,128)(2,1)}) %all-reduce.2.cloned.1.call-update) | async-done | bytes 2097168 | tf_op jit(solution)/shard_map/psum | solution.py:265
  438.0 3.2 copy.11
  441.2 0.0 copy-done
  441.2 1.3 copy.12
Async XLA Ops:
  7.2 263.5 %reduce-scatter.4.cloned.1.call-start = ((), (), s32[]{:S(2)}) async-start(), calls=%async_computation.4 | async-start | bytes 12582912 | tf_op jit(solution)/shard_map/reduce_scatter | solution.py:259
  118.6 8.8 %copy-start.1 = (bf16[2,2048,2048]{2,1,0:T(8,128)(2,1)S(1)}, bf16[2,2048,2048]{2,1,0:T(8,128)(2,1)}, u32[]{:S(2)}) copy-start(bf16[2,2048,2048]{2,1,0:T(8,128)(2,1)} %get-tuple-element.4) | copy-start | bytes 50331652
  118.6 10.6 %copy-start.2 = (bf16[3,2048,512]{2,1,0:T(8,128)(2,1)S(1)}, bf16[3,2048,512]{2,1,0:T(8,128)(2,1)}, u32[]{:S(2)}) copy-start(bf16[3,2048,512]{2,1,0:T(8,128)(2,1)} %get-tuple-element.5) | copy-start | bytes 18874372
  129.2 10.5 %copy-start.3 = (f32[2048,512]{1,0:T(8,128)}, f32[2048,512]{1,0:T(8,128)S(1)}, u32[]{:S(2)}) copy-start(f32[2048,512]{1,0:T(8,128)S(1)} %fusion) | copy-start | bytes 12582916
  139.7 2.0 copy-start.4
  171.1 146.1 %reduce-scatter.8.cloned.1.call-start = ((), (), s32[]{:S(2)}) async-start(), calls=%async_computation.7 | async-start | bytes 2621440 | tf_op jit(solution)/shard_map/reduce_scatter | solution.py:245
  183.0 197.8 %reduce-scatter.6.cloned.1.call-start = ((), (), s32[]{:S(2)}) async-start(), calls=%async_computation.5 | async-start | bytes 6291456 | tf_op jit(solution)/shard_map/reduce_scatter | solution.py:262
  270.6 143.8 %all-gather.2.cloned.1.call-start = ((), (), s32[]{:S(2)}) async-start(), calls=%async_computation.8 | async-start | bytes 3145728 | tf_op jit(solution)/shard_map/all_gather | solution.py:252
  344.6 93.4 %all-reduce.2.cloned.1.call-start = ((), (), s32[]{:S(2)}) async-start(), calls=%async_computation.6 | async-start | bytes 4194304 | tf_op jit(solution)/shard_map/psum | solution.py:265
  414.5 26.7 %copy-start = (f32[256,2048]{1,0:T(8,128)S(1)}, f32[256,2048]{1,0:T(8,128)}, u32[]{:S(2)}) copy-start(f32[256,2048]{1,0:T(8,128)} %all-gather.2.cloned.1.call-done) | copy-start | bytes 6291460
Sparse Core Ops, SparseCore 0:
  171.2 99.4 reduce-scatter.3
  273.5 43.6 reduce-scatter.7
  319.5 61.1 reduce-scatter.5
  382.7 31.7 all-gather.1
  416.6 21.3 all-reduce.1

commit v2 on v1

--- a/solution.py
+++ b/solution.py
@@ -208,6 +208,262 @@
     )(pieces, toks, cots)
 
 
+def reduce_kernel(
+    line, p_in, g_in, gi_out, gd_out,
+    r1, s1, rx, ry, s3, fin, u_in, d_in, u_out, d_out, gfin,
+    c_s, c_r, x_s, x_r, yy_s, yy_r, u_s, u_r, d_s, d_r, f_s, f_r, o_s, o_r, loc,
+):
+    r = lax.axis_index("rep")
+    f = lax.axis_index("fs")
+    core = lax.axis_index("tp")
+    z, y = f // 2, f % 2
+    rows = p_in.shape[0] // 4
+    cols = p_in.shape[1] // 2
+    side = cols // 2
+    width = g_in.shape[1]
+    zrows = g_in.shape[0] // line
+    frows = zrows // 2
+    up = {"fs": (f + 2) % (2 * line)}
+    dn = {"fs": (f + 2 * line - 2) % (2 * line)}
+    ypart = {"fs": f + 1 - 2 * y}
+    xpart = {"rep": 1 - r}
+    cpart = {"tp": 1 - core}
+
+    barrier = pltpu.get_barrier_semaphore()
+    for dev in (ypart, xpart, cpart, up, dn):
+        pl.semaphore_signal(barrier, inc=1, device_id=dev, device_id_type=MESH)
+    pl.semaphore_wait(barrier, 5)
+
+    def remote(src, dst, s, q, dev):
+        return pltpu.make_async_remote_copy(
+            src_ref=src, dst_ref=dst, send_sem=s, recv_sem=q,
+            device_id=dev, device_id_type=MESH,
+        )
+
+    def total(dst, terms, count, step=64):
+        @pl.loop(0, count // step)
+        def _(i):
+            at = pl.multiple_of(i * step, step)
+            value = None
+            for ref, row, col, wide in terms:
+                one = ref[pl.ds(row + at, step), pl.ds(col, wide)].astype(jnp.float32)
+                value = one if value is None else value + one
+            ref, row, col, wide = dst
+            ref[pl.ds(row + at, step), pl.ds(col, wide)] = value.astype(ref.dtype)
+
+    def slot(rr, yy):
+        return pl.multiple_of((2 * rr + yy) * rows, rows)
+
+    order = [(1 - r, 1 - y), (1 - r, y), (r, 1 - y), (r, y)]
+    my_col = pl.multiple_of(core * cols, cols)
+    its_col = pl.multiple_of((1 - core) * cols, cols)
+
+    def core_copy(i):
+        at = pl.ds(slot(*order[i]), rows)
+        return remote(p_in.at[at, pl.ds(its_col, cols)], r1.at[at, :], c_s.at[i], c_r.at[i], cpart)
+
+    def s1_half(i, second):
+        return s1.at[pl.ds(slot(*order[i]), rows), pl.ds(side if second else 0, side)]
+
+    def x_copy(i):
+        src = (s1_half(0, False), s1_half(1, False), s3.at[1])[i]
+        return remote(src, rx.at[i], x_s.at[i], x_r.at[i], xpart)
+
+    def y_copy(i):
+        src = (s1_half(0, True), s1_half(2, True), s3.at[0])[i]
+        return remote(src, ry.at[i], yy_s.at[i], yy_r.at[i], ypart)
+
+    def block(ref, zt):
+        return ref.at[pl.ds(zt * zrows, zrows), :]
+
+    def up_copy(zt, first):
+        return remote(block(g_in if first else u_out, zt), block(u_in, zt), u_s.at[zt], u_r.at[zt], up)
+
+    def dn_copy(zt, first):
+        return remote(block(g_in if first else d_out, zt), block(d_in, zt), d_s.at[zt], d_r.at[zt], dn)
+
+    def line_step(i):
+        zt = line - 1 - i
+        if zt > 0:
+            @pl.when((z > 0) & (z < zt))
+            def _():
+                up_copy(zt, False).wait_recv()
+                row = zt * zrows
+                total((u_out, row, 0, width), [(g_in, row, 0, width), (u_in, row, 0, width)], zrows)
+                up_copy(zt, False).start()
+
+            zd = i
+
+            @pl.when((z < line - 1) & (z > zd))
+            def _():
+                dn_copy(zd, False).wait_recv()
+                row = zd * zrows
+                total((d_out, row, 0, width), [(g_in, row, 0, width), (d_in, row, 0, width)], zrows)
+                dn_copy(zd, False).start()
+
+    for i in range(4):
+        core_copy(i).start()
+    for i in range(line - 1):
+        @pl.when(z == 0)
+        def _():
+            up_copy(line - 1 - i, True).start()
+
+        @pl.when(z == line - 1)
+        def _():
+            dn_copy(i, True).start()
+
+    for i in range(4):
+        core_copy(i).wait_recv()
+        row = slot(*order[i])
+        total((s1, row, 0, cols), [(p_in, row, my_col, cols), (r1, row, 0, cols)], rows)
+        if i in (0, 1):
+            x_copy(i).start()
+        if i == 0:
+            y_copy(0).start()
+        if i == 2:
+            y_copy(1).start()
+
+    line_step(0)
+    x_copy(0).wait_recv()
+    total((s3.at[0], 0, 0, side), [(s1, slot(r, 1 - y), 0, side), (rx.at[0], 0, 0, side)], rows)
+    y_copy(2).start()
+    y_copy(0).wait_recv()
+    total((s3.at[1], 0, 0, side), [(s1, slot(1 - r, y), side, side), (ry.at[0], 0, 0, side)], rows)
+    x_copy(2).start()
+    for i in range(1, line - 1):
+        line_step(i)
+
+    zrow = pl.multiple_of(z * zrows, zrows)
+
+    def here(ref):
+        return (ref, zrow, 0, width)
+
+    @pl.when(z == 0)
+    def _():
+        dn_copy(0, True).wait_recv()
+        total((gfin, 0, 0, width), [here(g_in), here(d_in)], zrows)
+
+    @pl.when(z == line - 1)
+    def _():
+        up_copy(line - 1, True).wait_recv()
+        total((gfin, 0, 0, width), [here(g_in), here(u_in)], zrows)
+
+    @pl.when((z > 0) & (z < line - 1))
+    def _():
+        remote(block(g_in, z), block(u_in, z), u_s.at[z], u_r.at[z], up).wait_recv()
+        remote(block(g_in, z), block(d_in, z), d_s.at[z], d_r.at[z], dn).wait_recv()
+        total((gfin, 0, 0, width), [here(g_in), here(u_in), here(d_in)], zrows)
+
+    def gcols(rr, yy):
+        return gd_out.at[:, pl.ds(pl.multiple_of((2 * rr + yy) * width, width), width)]
+
+    def grows(yy):
+        return gfin.at[pl.ds(pl.multiple_of(yy * frows, frows), frows), :]
+
+    def f_copy(i, landing):
+        if i == 0:
+            dst = gcols(r, 1 - y) if landing else gcols(r, y)
+            return remote(grows(1 - y), dst, f_s.at[0], f_r.at[0], ypart)
+        if i == 1:
+            dst = gcols(1 - r, y) if landing else gcols(r, y)
+            return remote(grows(y), dst, f_s.at[1], f_r.at[1], xpart)
+        dst = gcols(1 - r, 1 - y) if landing else gcols(r, 1 - y)
+        return remote(gcols(r, 1 - y), dst, f_s.at[2], f_r.at[2], xpart)
+
+    f_copy(0, False).start()
+    f_copy(1, False).start()
+    own_g = pltpu.make_async_copy(grows(y), gcols(r, y), loc.at[0])
+    own_g.start()
+
+    x_copy(1).wait_recv()
+    y_copy(2).wait_recv()
+    here_row = slot(r, y)
+    total(
+        (fin, 0, 0, side),
+        [(s1, here_row, 0, side), (rx.at[1], 0, 0, side), (ry.at[2], 0, 0, side)], rows,
+    )
+
+    def o_copy(i, landing):
+        base = (1 - core if landing else core) * cols + i * side
+        dst = gi_out.at[:, pl.ds(pl.multiple_of(base, side), side)]
+        return remote(fin.at[:, pl.ds(i * side, side)], dst, o_s.at[i], o_r.at[i], cpart)
+
+    def o_local(i):
+        base = pl.multiple_of(core * cols + i * side, side)
+        return pltpu.make_async_copy(
+            fin.at[:, pl.ds(i * side, side)], gi_out.at[:, pl.ds(base, side)], loc.at[1 + i]
+        )
+
+    o_copy(0, False).start()
+    o_local(0).start()
+    f_copy(0, True).wait_recv()
+    f_copy(2, False).start()
+    y_copy(1).wait_recv()
+    x_copy(2).wait_recv()
+    total(
+        (fin, 0, side, side),
+        [(s1, here_row, side, side), (ry.at[1], 0, 0, side), (rx.at[2], 0, 0, side)], rows,
+    )
+    o_copy(1, False).start()
+    o_local(1).start()
+
+    for i in range(4):
+        core_copy(i).wait_send()
+    for i in range(3):
+        x_copy(i).wait_send()
+        y_copy(i).wait_send()
+        f_copy(i, False).wait_send()
+    f_copy(1, True).wait_recv()
+    f_copy(2, True).wait_recv()
+    for i in range(2):
+        o_copy(i, True).wait_recv()
+        o_copy(i, False).wait_send()
+        o_local(i).wait()
+    own_g.wait()
+    for zt in range(line):
+        if zt > 0:
+            pl.when(z < zt)(lambda: up_copy(zt, True).wait_send())
+        if zt < line - 1:
+            pl.when(z > zt)(lambda: dn_copy(zt, True).wait_send())
+
+
+def reduced(part, grad_part):
+    line = lax.axis_size("fs") // 2
+    rows, cols = part.shape[0] // 4, part.shape[1] // 2
+    depth, width = grad_part.shape
+    kind = part.dtype
+    dma = pltpu.SemaphoreType.DMA
+    vmem = pl.BlockSpec(memory_space=pltpu.VMEM)
+    anyspec = pl.BlockSpec(memory_space=pl.ANY)
+    unit = pltpu.VMEM((3, rows, cols // 2), kind)
+    whole = pltpu.VMEM((depth, width), kind)
+    return pl.pallas_call(
+        functools.partial(reduce_kernel, line),
+        out_shape=(
+            jax.ShapeDtypeStruct((rows, 2 * cols), kind),
+            jax.ShapeDtypeStruct((depth // (2 * line), 4 * width), kind),
+        ),
+        in_specs=[vmem, vmem],
+        out_specs=(anyspec, anyspec),
+        scratch_shapes=[
+            pltpu.VMEM((4 * rows, cols), kind),
+            pltpu.VMEM((4 * rows, cols), kind),
+            unit, unit,
+            pltpu.VMEM((2, rows, cols // 2), kind),
+            pltpu.VMEM((rows, cols), kind),
+            whole, whole, whole, whole,
+            pltpu.VMEM((depth // line, width), kind),
+            dma((4,)), dma((4,)), dma((3,)), dma((3,)), dma((3,)), dma((3,)),
+            dma((line,)), dma((line,)), dma((line,)), dma((line,)),
+            dma((3,)), dma((3,)), dma((2,)), dma((2,)), dma((3,)),
+        ],
+        compiler_params=pltpu.CompilerParams(
+            collective_id=1, has_side_effects=True, vmem_limit_bytes=56 * 2**20
+        ),
+        name="reduce_all",
+    )(part, grad_part)
+
+
 def on_device(inputs, cotangent, gate_weight, up_weight, down_weight):
     tok_rows = inputs.shape[0]
     fs_size = lax.axis_size("fs")
@@ -242,6 +498,17 @@
     grad_part = lax.dot_general(
         tokens[1], hidden, contract_tok, preferred_element_type=jnp.float32
     )
+    part = lax.dot_general(
+        grad_gate, gate_full, contract, preferred_element_type=jnp.float32
+    )
+    part = part + lax.dot_general(
+        grad_up, up_full, contract, preferred_element_type=jnp.float32
+    )
+    if lax.axis_size("tp") == 2:
+        grad_input, grad_down = reduced(
+            part.astype(jnp.bfloat16), grad_part.astype(jnp.bfloat16)
+        )
+        return (grad_input, grad_down.astype(jnp.float32) * grad_scale)
     shard = lax.psum_scatter(
         grad_part.astype(jnp.bfloat16), "fs", scatter_dimension=0, tiled=True,
         axis_index_groups=lines,
@@ -250,12 +517,6 @@
         shard, "fs", split_axis=0, concat_axis=1, tiled=True, axis_index_groups=pairs
     )
     grad_down = lax.all_gather(shard, "rep", axis=1, tiled=True)
-    part = lax.dot_general(
-        grad_gate, gate_full, contract, preferred_element_type=jnp.float32
-    )
-    part = part + lax.dot_general(
-        grad_up, up_full, contract, preferred_element_type=jnp.float32
-    )
     part = lax.psum_scatter(
         part.astype(jnp.bfloat16), "rep", scatter_dimension=0, tiled=True
     )

time: 449 us -> 248 us (0.55)
  waiting for transfers between devices: 228 us -> 0 us
  Pallas kernels: 108 us -> 172 us
  blocking collectives: 25.1 us -> 0 us
  between operations: 13.9 us -> 0.7 us
  local copies, waits for them, and re-layouts: 12.8 us -> 4.78 us
  matrix products: 59.3 us -> 65 us
    reduce_scatter x3 -> x0, waiting for transfers between devices: 170 us -> none  [the longest x1 87.6 us: on_device(): lax.psum_scatter(part.astype(jnp.bfloat16), 'rep', scatter_dimension=0, t...]
    pallas_call x0 -> x1, Pallas kernels: none -> 64.8 us  [reduced(): pl.pallas_call(functools.partial(reduce_kernel, line), out_shape=(jax.Sha...]
    all_gather x1 -> x0, waiting for transfers between devices: 33.7 us -> none  [on_device(): grad_down = lax.all_gather(shard, 'rep', axis=1, tiled=True)]
    all_to_all x1 -> x0, blocking collectives: 25.1 us -> none  [on_device(): lax.all_to_all(shard, 'fs', split_axis=0, concat_axis=1, tiled=True, axis...]
    psum x1 -> x0, waiting for transfers between devices: 23.5 us -> none  [on_device(): grad_input = lax.psum(part, 'tp')]
    unnamed x12 -> x7, local copies, waits for them, and re-layouts: 9.4 us -> 2.44 us
  transfers between devices with their start and end apart: 5 -> 0, of which waited for: 5 -> 0; matrix products, arithmetic and copies ran while one was open for 3% -> 0% of each run, Pallas kernels for 0% -> 0%
where the time goes in v2:
time: 248 us; the launch traced here: 247 us
  Pallas kernels  172 us (69%)
  matrix products  65 us (26%)
  local copies, waits for them, and re-layouts  4.78 us (2%)
  other arithmetic  4.4 us (2%)
    pallas_call x1, Pallas kernels, gather(): pl.pallas_call(functools.partial(gather_kernel, line, parts), out_shape=(...  108 us
    pallas_call x1, Pallas kernels, reduced(): pl.pallas_call(functools.partial(reduce_kernel, line), out_shape=(jax.Sha...  64.8 us
    dot_general x1, matrix products, on_device(): lax.dot_general(grad_up, up_full, contract, preferred_element_type=jnp.fl...  16.8 us
    dot_general x1, matrix products, on_device(): lax.dot_general(grad_gate, gate_full, contract, preferred_element_type=jn...  15.6 us
    dot_general x1, matrix products, on_device(): up_val = jnp.dot(tokens[0], up_full, preferred_element_type=jnp.float32)  9.09 us
    dot_general x1, matrix products, on_device(): lax.dot_general(tokens[1], hidden, contract_tok, preferred_element_type=j...  8.27 us
    dot_general x1, matrix products, on_device(): gate_val = jnp.dot(tokens[0], gate_full, preferred_element_type=jnp.float32)  7.7 us
    dot_general x1, matrix products, on_device(): jnp.dot(tokens[1], down_full, preferred_element_type=jnp.float32)  7.57 us

profile of v2, /device:TPU:0, one launch (start us, length us, event | category | flops | bytes accessed | tf_op | source)
XLA Modules:
  0.0 247.2 jit_solution(12205950522653946203)
XLA Ops:
  0.6 1.1 dynamic-slice_bitcast_fusion.5
  1.7 1.3 dynamic-slice_bitcast_fusion.3
  3.0 0.1 maximum_bitcast_fusion
  3.1 0.1 maximum_bitcast_fusion.1
  3.2 1.3 pad_maximum_fusion.pieces
  4.5 107.5 %gather_all.1 = (bf16[3,2048,512]{2,1,0:T(8,128)(2,1)}, bf16[2,2048,2048]{2,1,0:T(8,128)(2,1)}) custom-call(bf16[2,3,256,512]{3,2,1,0:T(8,128)(2,1)} %pad_maximum_fusion.pieces, bf16[512,2048]{1,0:T(8,128)(2,1)} %toks.1, bf16[512,2048]{1,0:T(8,128)(2,1)} %cots.1), custom_call_target="tpu_custom_call" | custom-call | tf_op jit(solution)/shard_map/gather_all/pallas_call | solution.py:190
  112.0 0.0 copy-start.1
  112.0 7.7 %fusion = f32[2048,512]{1,0:T(8,128)S(1)} fusion(bf16[2,2048,2048]{2,1,0:T(8,128)(2,1)} %get-tuple-element.6, bf16[3,2048,512]{2,1,0:T(8,128)(2,1)} %get-tuple-element.7), kind=kOutput, calls=%fused_computation.1 | convolution fusion | flops 4294967296 | bytes 14680064 | tf_op jit(solution)/shard_map/dot_general | solution.py:485
  119.7 1.1 copy-done.1
  120.8 0.0 copy-start.2
  120.8 9.1 %fusion.2 = f32[2048,512]{1,0:T(8,128)} fusion(bf16[2,2048,2048]{2,1,0:T(8,128)(2,1)S(1)} %copy-done.1, bf16[3,2048,512]{2,1,0:T(8,128)(2,1)} %get-tuple-element.7), kind=kOutput, calls=%fused_computation.3 | convolution fusion | flops 4294967296 | bytes 14680064 | tf_op jit(solution)/shard_map/dot_general | solution.py:486
  129.9 8.3 %fusion.13.g_in = bf16[2048,512]{1,0:T(8,128)(2,1)} fusion(bf16[2,2048,2048]{2,1,0:T(8,128)(2,1)S(1)} %copy-done.1, f32[2048,512]{1,0:T(8,128)} %fusion.2, f32[2048,512]{1,0:T(8,128)S(1)} %fusion), kind=kOutput, calls=%fused_computation.18 | convolution fusion | flops 4302307328 | bytes 18874368 | tf_op jit(solution)/shard_map/dot_general | solution.py:498
  138.2 7.6 %fusion.6 = f32[2048,512]{1,0:T(8,128)} fusion(bf16[2,2048,2048]{2,1,0:T(8,128)(2,1)S(1)} %copy-done.1, bf16[3,2048,512]{2,1,0:T(8,128)(2,1)} %get-tuple-element.7), kind=kOutput, calls=%fused_computation.7 | convolution fusion | flops 4294967296 | bytes 14680064 | tf_op jit(solution)/shard_map/dot_general | solution.py:487
  145.8 0.0 copy-done.2
  145.8 15.6 %fusion.16 = f32[2048,2048]{1,0:T(8,128)} fusion(f32[2048,512]{1,0:T(8,128)S(1)} %fusion, f32[2048,512]{1,0:T(8,128)} %fusion.6, f32[2048,512]{1,0:T(8,128)} %fusion.2, bf16[3,2048,512]{2,1,0:T(8,128)(2,1)} %get-tuple-element.7), kind=kOutput, calls=%fused_computation.19 | convolution fusion | flops 4305453056 | bytes 31457280 | tf_op jit(solution)/shard_map/dot_general | solution.py:501
  161.4 16.8 %add_convert_fusion.p_in = bf16[2048,2048]{1,0:T(8,128)(2,1)} fusion(f32[2048,2048]{1,0:T(8,128)} %fusion.16, f32[2048,512]{1,0:T(8,128)} %fusion.6, bf16[3,2048,512]{2,1,0:T(8,128)(2,1)} %get-tuple-element.7, f32[2048,512]{1,0:T(8,128)} %copy-done.2), kind=kOutput, calls=%fused_computation | convolution fusion | flops 4309647360 | bytes 35651584 | tf_op jit(solution)/shard_map/dot_general | solution.py:504
  178.2 64.8 %reduce_all.1 = (bf16[512,2048]{1,0:T(8,128)(2,1)}, bf16[256,2048]{1,0:T(8,128)(2,1)}) custom-call(bf16[2048,2048]{1,0:T(8,128)(2,1)} %add_convert_fusion.p_in, bf16[2048,512]{1,0:T(8,128)(2,1)} %fusion.13.g_in), custom_call_target="tpu_custom_call" | custom-call | tf_op jit(solution)/shard_map/reduce_all/pallas_call | solution.py:440
  243.0 0.0 copy-start
  243.0 2.9 %convert_multiply_fusion = f32[256,2048]{1,0:T(8,128)} fusion(bf16[256,2048]{1,0:T(8,128)(2,1)} %get-tuple-element.9), kind=kLoop, calls=%fused_computation.25 | loop fusion | flops 1048576 | bytes 3145728 | tf_op jit(solution)/shard_map/mul | solution.py:511
  245.9 0.0 copy-done
  245.9 1.3 copy.8
Async XLA Ops:
  112.0 8.8 %copy-start.1 = (bf16[2,2048,2048]{2,1,0:T(8,128)(2,1)S(1)}, bf16[2,2048,2048]{2,1,0:T(8,128)(2,1)}, u32[]{:S(2)}) copy-start(bf16[2,2048,2048]{2,1,0:T(8,128)(2,1)} %get-tuple-element.6) | copy-start | bytes 50331652
  120.8 24.9 %copy-start.2 = (f32[2048,512]{1,0:T(8,128)}, f32[2048,512]{1,0:T(8,128)S(1)}, u32[]{:S(2)}) copy-start(f32[2048,512]{1,0:T(8,128)S(1)} %fusion) | copy-start | bytes 12582916
  243.0 3.0 %copy-start = (bf16[512,2048]{1,0:T(8,128)(2,1)S(1)}, bf16[512,2048]{1,0:T(8,128)(2,1)}, u32[]{:S(2)}) copy-start(bf16[512,2048]{1,0:T(8,128)(2,1)} %get-tuple-element.20) | copy-start | bytes 6291460

commit v3 on v2

--- a/solution.py
+++ b/solution.py
@@ -12,7 +12,7 @@
 
 
 def gather_kernel(
-    line, parts, pieces, toks, cots, w_out, t_out, w_tmp, t_tmp,
+    line, units, gu_pieces, d_pieces, toks, cots, gu_out, d_out, t_out, gu_tmp, d_tmp, t_tmp,
     up_s, up_r, dn_s, dn_r, y_s, y_r, tok_s, tok_r, d2d_s, d2d_r, loc, loc2,
 ):
     r = lax.axis_index("rep")
@@ -21,8 +21,8 @@
     z, y = f // 2, f % 2
     rows = toks.shape[0]
     half = rows // 2
-    wrows = pieces.shape[2]
-    per = pieces.shape[1] // parts
+    wrows = gu_pieces.shape[1]
+    parts = len(units)
     has_up, has_dn = z < line - 1, z > 0
     up = {"fs": (f + 2) % (2 * line)}
     dn = {"fs": (f + 2 * line - 2) % (2 * line)}
@@ -48,10 +48,12 @@
 
     def wblk(k, zz, yy):
         row = pl.multiple_of((2 * zz + yy) * wrows, wrows)
-        return w_out.at[pl.ds(k * per, per), pl.ds(row, wrows), :]
+        which, col, wide = units[k]
+        return (gu_out, d_out)[which].at[pl.ds(row, wrows), pl.ds(col, wide)]
 
     def own(k, yy):
-        return pieces.at[yy, pl.ds(k * per, per)]
+        which, col, wide = units[k]
+        return (gu_pieces, d_pieces)[which].at[yy, :, pl.ds(col, wide)]
 
     def to_y(k):
         return remote(own(k, 1 - y), wblk(k, z, y), y_s.at[k], y_r.at[k], ypart)
@@ -118,14 +120,16 @@
         return remote(blk, blk, d2d_s.at[i], d2d_r.at[i], cpart)
 
     loads = [
-        pltpu.make_async_copy(pieces.at[y], w_tmp, loc.at[0]),
+        pltpu.make_async_copy(gu_pieces.at[y], gu_tmp, loc.at[0]),
+        pltpu.make_async_copy(d_pieces.at[y], d_tmp, loc.at[3]),
         pltpu.make_async_copy(toks, t_tmp.at[0], loc.at[1]),
         pltpu.make_async_copy(cots, t_tmp.at[1], loc.at[2]),
     ]
     trow = pl.multiple_of((2 * r + y) * rows, rows)
     wrow = pl.multiple_of(f * wrows, wrows)
     stores = [
-        pltpu.make_async_copy(w_tmp, w_out.at[:, pl.ds(wrow, wrows), :], loc2.at[0]),
+        pltpu.make_async_copy(gu_tmp, gu_out.at[pl.ds(wrow, wrows), :], loc2.at[0]),
+        pltpu.make_async_copy(d_tmp, d_out.at[pl.ds(wrow, wrows), :], loc2.at[3]),
         pltpu.make_async_copy(t_tmp.at[0], t_out.at[0, pl.ds(trow, rows), :], loc2.at[1]),
         pltpu.make_async_copy(t_tmp.at[1], t_out.at[1, pl.ds(trow, rows), :], loc2.at[2]),
     ]
@@ -180,32 +184,39 @@
         store.wait()
 
 
-def gather(pieces, toks, cots):
+def gather(gu_pieces, d_pieces, toks, cots):
     line = lax.axis_size("fs") // 2
-    kinds, wrows, width = pieces.shape[1:]
-    parts = kinds if line <= 4 else 1
+    _, wrows, width = d_pieces.shape
+    units = [(0, 0, 2 * width), (1, 0, width)]
+    if line <= 4:
+        units = [(0, 0, width), (0, width, width), (1, 0, width)]
+    parts = len(units)
+    depth = 2 * line * wrows
+    kind = d_pieces.dtype
     dma = pltpu.SemaphoreType.DMA
     zsem = dma((line - 1, 2, parts))
     anyspec = pl.BlockSpec(memory_space=pl.ANY)
     return pl.pallas_call(
-        functools.partial(gather_kernel, line, parts),
+        functools.partial(gather_kernel, line, units),
         out_shape=(
-            jax.ShapeDtypeStruct((kinds, 2 * line * wrows, width), pieces.dtype),
+            jax.ShapeDtypeStruct((depth, 2 * width), kind),
+            jax.ShapeDtypeStruct((depth, width), kind),
             jax.ShapeDtypeStruct((2, 4 * toks.shape[0], toks.shape[1]), toks.dtype),
         ),
-        in_specs=[anyspec] * 3,
-        out_specs=(anyspec, anyspec),
+        in_specs=[anyspec] * 4,
+        out_specs=(anyspec,) * 3,
         scratch_shapes=[
-            pltpu.VMEM(pieces.shape[1:], pieces.dtype),
+            pltpu.VMEM(gu_pieces.shape[1:], kind),
+            pltpu.VMEM(d_pieces.shape[1:], kind),
             pltpu.VMEM((2,) + toks.shape, toks.dtype),
             zsem, zsem, zsem, zsem,
             dma((parts,)), dma((parts,)),
             dma((6,)), dma((6,)), dma((6,)), dma((6,)),
-            dma((3,)), dma((3,)),
+            dma((4,)), dma((4,)),
         ],
         compiler_params=pltpu.CompilerParams(collective_id=0, has_side_effects=True),
         name="gather_all",
-    )(pieces, toks, cots)
+    )(gu_pieces, d_pieces, toks, cots)
 
 
 def reduce_kernel(
@@ -474,16 +485,20 @@
     r = lax.axis_index("rep")
     y = lax.axis_index("fs") % 2
 
-    def piece(side):
-        return jnp.stack([
-            lax.dynamic_slice_in_dim(weight, (2 * r + side) * width, width, 1)
-            for weight in (gate_weight, up_weight, down_weight)
-        ])
-
-    weights, tokens = gather(jnp.stack([piece(0), piece(1)]), inputs, cotangent)
-    gate_full, up_full, down_full = weights[0], weights[1], weights[2]
-    gate_val = jnp.dot(tokens[0], gate_full, preferred_element_type=jnp.float32)
-    up_val = jnp.dot(tokens[0], up_full, preferred_element_type=jnp.float32)
+    def piece(weight, side):
+        return lax.dynamic_slice_in_dim(weight, (2 * r + side) * width, width, 1)
+
+    def both(side):
+        return jnp.concatenate([piece(gate_weight, side), piece(up_weight, side)], axis=1)
+
+    gate_up, down_full, tokens = gather(
+        jnp.stack([both(0), both(1)]),
+        jnp.stack([piece(down_weight, 0), piece(down_weight, 1)]),
+        inputs,
+        cotangent,
+    )
+    gate_up_val = jnp.dot(tokens[0], gate_up, preferred_element_type=jnp.float32)
+    gate_val, up_val = gate_up_val[:, :width], gate_up_val[:, width:]
     grad_hidden = jnp.dot(tokens[1], down_full, preferred_element_type=jnp.float32)
     sigmoid_gate = jax.nn.sigmoid(gate_val)
     active = gate_val * sigmoid_gate
@@ -499,10 +514,8 @@
         tokens[1], hidden, contract_tok, preferred_element_type=jnp.float32
     )
     part = lax.dot_general(
-        grad_gate, gate_full, contract, preferred_element_type=jnp.float32
-    )
-    part = part + lax.dot_general(
-        grad_up, up_full, contract, preferred_element_type=jnp.float32
+        jnp.concatenate([grad_gate, grad_up], axis=1), gate_up, contract,
+        preferred_element_type=jnp.float32,
     )
     if lax.axis_size("tp") == 2:
         grad_input, grad_down = reduced(

time: 248 us -> 230 us (0.927)
  matrix products: 65 us -> 48.4 us
    dot_general x4 -> x2, matrix products: 49.2 us -> 28.7 us  [the longest x1 14.7 us: on_device(): jnp.dot(tokens[0], gate_up, preferred_element_type=jnp.float32)]
where the time goes in v3:
time: 230 us
  Pallas kernels  172 us (75%)
  matrix products  48.4 us (21%)
  other arithmetic  4.98 us (2%)
  local copies, waits for them, and re-layouts  3.67 us (2%)
    pallas_call x1, Pallas kernels, gather(): pl.pallas_call(functools.partial(gather_kernel, line, units), out_shape=(...  108 us
    pallas_call x1, Pallas kernels, reduced(): pl.pallas_call(functools.partial(reduce_kernel, line), out_shape=(jax.Sha...  64.8 us
    dot_general x1, matrix products, on_device(): jnp.dot(tokens[0], gate_up, preferred_element_type=jnp.float32)  14.7 us
    dot_general x1, matrix products, on_device(): lax.dot_general(jnp.concatenate([grad_gate, grad_up], axis=1), gate_up, c...  14 us
    dot_general x1, matrix products, on_device(): lax.dot_general(tokens[1], hidden, contract_tok, preferred_element_type=j...  9.96 us
    dot_general x1, matrix products, on_device(): jnp.dot(tokens[1], down_full, preferred_element_type=jnp.float32)  9.82 us

profile of v3, /device:TPU:0, one launch (start us, length us, event | category | flops | bytes accessed | tf_op | source)
XLA Modules:
  0.0 230.1 jit_solution(8735537507697501958)
XLA Ops:
  0.6 1.1 dynamic-slice_bitcast_fusion.1
  1.7 0.8 pad_maximum_fusion.1.d_pieces
  2.6 1.3 constant_dynamic-slice_fusion.2
  3.8 0.1 maximum_bitcast_fusion
  3.9 0.1 maximum_bitcast_fusion.1
  4.0 1.1 pad_maximum_fusion.gu_pieces
  5.0 107.6 %gather_all.1 = (bf16[2048,1024]{1,0:T(8,128)(2,1)}, bf16[2048,512]{1,0:T(8,128)(2,1)}, bf16[2,2048,2048]{2,1,0:T(8,128)(2,1)}) custom-call(bf16[2,256,1024]{2,1,0:T(8,128)(2,1)} %pad_maximum_fusion.gu_pieces, bf16[2,256,512]{2,1,0:T(8,128)(2,1)} %pad_maximum_fusion.1.d_pieces, bf16[512,2048]{1,0:T(8,128)(2,1)} %toks.1, bf16[512,2048]{1,0:T(8,128)(2,1)} %cots.1), custom_call_target="tpu_custom_call" | custom-call | tf_op jit(solution)/shard_map/gather_all/pallas_call | solution.py:199
  112.6 0.0 copy-start.1
  112.6 14.7 %fusion = f32[2048,1024]{0,1:T(8,128)} fusion(bf16[2048,1024]{1,0:T(8,128)(2,1)} %get-tuple-element.9, bf16[2,2048,2048]{2,1,0:T(8,128)(2,1)} %get-tuple-element.7), kind=kOutput, calls=%fused_computation | convolution fusion | flops 8589934592 | bytes 20971520 | tf_op jit(solution)/shard_map/dot_general | solution.py:500
  127.3 0.0 copy-done.1
  127.3 0.0 copy-start.2
  127.3 10.0 %fusion.13.g_in = bf16[2048,512]{1,0:T(8,128)(2,1)} fusion(bf16[2,2048,2048]{2,1,0:T(8,128)(2,1)S(1)} %copy-done.1, f32[2048,1024]{0,1:T(8,128)} %fusion), kind=kOutput, calls=%fused_computation.18 | convolution fusion | flops 4302307328 | bytes 18874368 | tf_op jit(solution)/shard_map/dot_general | solution.py:513
  137.3 0.0 copy-done.2
  137.3 9.8 %multiply_convert_fusion.2 = (bf16[2048,512]{0,1:T(8,128)(2,1)}, bf16[2048,512]{0,1:T(8,128)(2,1)}) fusion(f32[2048,1024]{0,1:T(8,128)} %fusion, bf16[2048,512]{1,0:T(8,128)(2,1)S(1)} %copy-done.2, bf16[2,2048,2048]{2,1,0:T(8,128)(2,1)S(1)} %copy-done.1), kind=kOutput, calls=%fused_computation.15 | convolution fusion | flops 4308598784 | bytes 23068672 | tf_op jit(solution)/shard_map/dot_general | solution.py:502
  147.1 14.0 %convolution_convert_fusion.p_in = bf16[2048,2048]{1,0:T(8,128)(2,1)} fusion(bf16[2048,1024]{1,0:T(8,128)(2,1)} %get-tuple-element.9, bf16[2048,512]{0,1:T(8,128)(2,1)} %get-tuple-element.13, bf16[2048,512]{0,1:T(8,128)(2,1)} %get-tuple-element.12), kind=kOutput, calls=%fused_computation.7 | convolution fusion | flops 8602517504 | bytes 16777216 | tf_op jit(solution)/shard_map/dot_general | solution.py:516
  161.0 64.8 %reduce_all.1 = (bf16[512,2048]{1,0:T(8,128)(2,1)}, bf16[256,2048]{1,0:T(8,128)(2,1)}) custom-call(bf16[2048,2048]{1,0:T(8,128)(2,1)} %convolution_convert_fusion.p_in, bf16[2048,512]{1,0:T(8,128)(2,1)} %fusion.13.g_in), custom_call_target="tpu_custom_call" | custom-call | tf_op jit(solution)/shard_map/reduce_all/pallas_call | solution.py:451
  225.8 0.0 copy-start
  225.8 2.9 %convert_multiply_fusion = f32[256,2048]{1,0:T(8,128)} fusion(bf16[256,2048]{1,0:T(8,128)(2,1)} %get-tuple-element.11), kind=kLoop, calls=%fused_computation.19 | loop fusion | flops 1048576 | bytes 3145728 | tf_op jit(solution)/shard_map/mul | solution.py:524
  228.8 0.0 copy-done
  228.8 1.3 copy.8
Async XLA Ops:
  112.6 14.7 %copy-start.1 = (bf16[2,2048,2048]{2,1,0:T(8,128)(2,1)S(1)}, bf16[2,2048,2048]{2,1,0:T(8,128)(2,1)}, u32[]{:S(2)}) copy-start(bf16[2,2048,2048]{2,1,0:T(8,128)(2,1)} %get-tuple-element.7) | copy-start | bytes 50331652
  127.3 10.0 %copy-start.2 = (bf16[2048,512]{1,0:T(8,128)(2,1)S(1)}, bf16[2048,512]{1,0:T(8,128)(2,1)}, u32[]{:S(2)}) copy-start(bf16[2048,512]{1,0:T(8,128)(2,1)} %get-tuple-element.8) | copy-start | bytes 6291460
  225.8 3.0 %copy-start = (bf16[512,2048]{1,0:T(8,128)(2,1)S(1)}, bf16[512,2048]{1,0:T(8,128)(2,1)}, u32[]{:S(2)}) copy-start(bf16[512,2048]{1,0:T(8,128)(2,1)} %get-tuple-element.24) | copy-start | bytes 6291460

commit v4 on v3

--- a/solution.py
+++ b/solution.py
@@ -12,7 +12,7 @@
 
 
 def gather_kernel(
-    line, units, gu_pieces, d_pieces, toks, cots, gu_out, d_out, t_out, gu_tmp, d_tmp, t_tmp,
+    line, units, gate_w, up_w, down_w, toks, cots, gu_out, d_out, t_out, w_tmp, t_tmp,
     up_s, up_r, dn_s, dn_r, y_s, y_r, tok_s, tok_r, d2d_s, d2d_r, loc, loc2,
 ):
     r = lax.axis_index("rep")
@@ -21,7 +21,8 @@
     z, y = f // 2, f % 2
     rows = toks.shape[0]
     half = rows // 2
-    wrows = gu_pieces.shape[1]
+    wrows = gate_w.shape[0]
+    width = gate_w.shape[1] // 4
     parts = len(units)
     has_up, has_dn = z < line - 1, z > 0
     up = {"fs": (f + 2) % (2 * line)}
@@ -52,8 +53,8 @@
         return (gu_out, d_out)[which].at[pl.ds(row, wrows), pl.ds(col, wide)]
 
     def own(k, yy):
-        which, col, wide = units[k]
-        return (gu_pieces, d_pieces)[which].at[yy, :, pl.ds(col, wide)]
+        col = pl.multiple_of((2 * r + yy) * width, width)
+        return (gate_w, up_w, down_w)[k].at[:, pl.ds(col, width)]
 
     def to_y(k):
         return remote(own(k, 1 - y), wblk(k, z, y), y_s.at[k], y_r.at[k], ypart)
@@ -120,16 +121,17 @@
         return remote(blk, blk, d2d_s.at[i], d2d_r.at[i], cpart)
 
     loads = [
-        pltpu.make_async_copy(gu_pieces.at[y], gu_tmp, loc.at[0]),
-        pltpu.make_async_copy(d_pieces.at[y], d_tmp, loc.at[3]),
+        pltpu.make_async_copy(own(0, y), w_tmp.at[0], loc.at[0]),
+        pltpu.make_async_copy(own(1, y), w_tmp.at[1], loc.at[3]),
+        pltpu.make_async_copy(own(2, y), w_tmp.at[2], loc.at[4]),
         pltpu.make_async_copy(toks, t_tmp.at[0], loc.at[1]),
         pltpu.make_async_copy(cots, t_tmp.at[1], loc.at[2]),
     ]
     trow = pl.multiple_of((2 * r + y) * rows, rows)
-    wrow = pl.multiple_of(f * wrows, wrows)
     stores = [
-        pltpu.make_async_copy(gu_tmp, gu_out.at[pl.ds(wrow, wrows), :], loc2.at[0]),
-        pltpu.make_async_copy(d_tmp, d_out.at[pl.ds(wrow, wrows), :], loc2.at[3]),
+        pltpu.make_async_copy(w_tmp.at[0], wblk(0, z, y), loc2.at[0]),
+        pltpu.make_async_copy(w_tmp.at[1], wblk(1, z, y), loc2.at[3]),
+        pltpu.make_async_copy(w_tmp.at[2], wblk(2, z, y), loc2.at[4]),
         pltpu.make_async_copy(t_tmp.at[0], t_out.at[0, pl.ds(trow, rows), :], loc2.at[1]),
         pltpu.make_async_copy(t_tmp.at[1], t_out.at[1, pl.ds(trow, rows), :], loc2.at[2]),
     ]
@@ -184,15 +186,13 @@
         store.wait()
 
 
-def gather(gu_pieces, d_pieces, toks, cots):
+def gather(gate_w, up_w, down_w, toks, cots):
     line = lax.axis_size("fs") // 2
-    _, wrows, width = d_pieces.shape
-    units = [(0, 0, 2 * width), (1, 0, width)]
-    if line <= 4:
-        units = [(0, 0, width), (0, width, width), (1, 0, width)]
+    wrows, width = gate_w.shape[0], gate_w.shape[1] // 4
+    units = [(0, 0, width), (0, width, width), (1, 0, width)]
     parts = len(units)
     depth = 2 * line * wrows
-    kind = d_pieces.dtype
+    kind = gate_w.dtype
     dma = pltpu.SemaphoreType.DMA
     zsem = dma((line - 1, 2, parts))
     anyspec = pl.BlockSpec(memory_space=pl.ANY)
@@ -203,25 +203,24 @@
             jax.ShapeDtypeStruct((depth, width), kind),
             jax.ShapeDtypeStruct((2, 4 * toks.shape[0], toks.shape[1]), toks.dtype),
         ),
-        in_specs=[anyspec] * 4,
+        in_specs=[anyspec] * 5,
         out_specs=(anyspec,) * 3,
         scratch_shapes=[
-            pltpu.VMEM(gu_pieces.shape[1:], kind),
-            pltpu.VMEM(d_pieces.shape[1:], kind),
+            pltpu.VMEM((parts, wrows, width), kind),
             pltpu.VMEM((2,) + toks.shape, toks.dtype),
             zsem, zsem, zsem, zsem,
             dma((parts,)), dma((parts,)),
             dma((6,)), dma((6,)), dma((6,)), dma((6,)),
-            dma((4,)), dma((4,)),
+            dma((5,)), dma((5,)),
         ],
         compiler_params=pltpu.CompilerParams(collective_id=0, has_side_effects=True),
         name="gather_all",
-    )(gu_pieces, d_pieces, toks, cots)
+    )(gate_w, up_w, down_w, toks, cots)
 
 
 def reduce_kernel(
     line, p_in, g_in, gi_out, gd_out,
-    r1, s1, rx, ry, s3, fin, u_in, d_in, u_out, d_out, gfin,
+    p_tmp, r1, s1, rx, ry, s3, fin, u_in, d_in, u_out, d_out, gfin,
     c_s, c_r, x_s, x_r, yy_s, yy_r, u_s, u_r, d_s, d_r, f_s, f_r, o_s, o_r, loc,
 ):
     r = lax.axis_index("rep")
@@ -312,8 +311,13 @@
                 total((d_out, row, 0, width), [(g_in, row, 0, width), (d_in, row, 0, width)], zrows)
                 dn_copy(zd, False).start()
 
+    def p_load(i):
+        at = pl.ds(slot(*order[i]), rows)
+        return pltpu.make_async_copy(p_in.at[at, pl.ds(my_col, cols)], p_tmp.at[at, :], loc.at[3 + i])
+
     for i in range(4):
         core_copy(i).start()
+        p_load(i).start()
     for i in range(line - 1):
         @pl.when(z == 0)
         def _():
@@ -324,9 +328,10 @@
             dn_copy(i, True).start()
 
     for i in range(4):
+        p_load(i).wait()
         core_copy(i).wait_recv()
         row = slot(*order[i])
-        total((s1, row, 0, cols), [(p_in, row, my_col, cols), (r1, row, 0, cols)], rows)
+        total((s1, row, 0, cols), [(p_tmp, row, 0, cols), (r1, row, 0, cols)], rows)
         if i in (0, 1):
             x_copy(i).start()
         if i == 0:
@@ -454,9 +459,10 @@
             jax.ShapeDtypeStruct((rows, 2 * cols), kind),
             jax.ShapeDtypeStruct((depth // (2 * line), 4 * width), kind),
         ),
-        in_specs=[vmem, vmem],
+        in_specs=[anyspec, vmem],
         out_specs=(anyspec, anyspec),
         scratch_shapes=[
+            pltpu.VMEM((4 * rows, cols), kind),
             pltpu.VMEM((4 * rows, cols), kind),
             pltpu.VMEM((4 * rows, cols), kind),
             unit, unit,
@@ -466,7 +472,7 @@
             pltpu.VMEM((depth // line, width), kind),
             dma((4,)), dma((4,)), dma((3,)), dma((3,)), dma((3,)), dma((3,)),
             dma((line,)), dma((line,)), dma((line,)), dma((line,)),
-            dma((3,)), dma((3,)), dma((2,)), dma((2,)), dma((3,)),
+            dma((3,)), dma((3,)), dma((2,)), dma((2,)), dma((7,)),
         ],
         compiler_params=pltpu.CompilerParams(
             collective_id=1, has_side_effects=True, vmem_limit_bytes=56 * 2**20
@@ -482,20 +488,8 @@
     contract = (((1,), (1,)), ((), ()))
     contract_tok = (((0,), (0,)), ((), ()))
     width = gate_weight.shape[1] // 4
-    r = lax.axis_index("rep")
-    y = lax.axis_index("fs") % 2
-
-    def piece(weight, side):
-        return lax.dynamic_slice_in_dim(weight, (2 * r + side) * width, width, 1)
-
-    def both(side):
-        return jnp.concatenate([piece(gate_weight, side), piece(up_weight, side)], axis=1)
-
     gate_up, down_full, tokens = gather(
-        jnp.stack([both(0), both(1)]),
-        jnp.stack([piece(down_weight, 0), piece(down_weight, 1)]),
-        inputs,
-        cotangent,
+        gate_weight, up_weight, down_weight, inputs, cotangent
     )
     gate_up_val = jnp.dot(tokens[0], gate_up, preferred_element_type=jnp.float32)
     gate_val, up_val = gate_up_val[:, :width], gate_up_val[:, width:]

time: 230 us -> 224 us (0.974)
  local copies, waits for them, and re-layouts: 3.67 us -> 1.33 us
    pallas_call x1, Pallas kernels: 64.8 us -> 62.4 us  [reduced(): pl.pallas_call(functools.partial(reduce_kernel, line), out_shape=(jax.Sha...]
where the time goes in v4:
time: 224 us; the launch traced here: 223 us
  Pallas kernels  170 us (76%)
  matrix products  48.5 us (22%)
  other arithmetic  2.95 us (1%)
    pallas_call x1, Pallas kernels, gather(): pl.pallas_call(functools.partial(gather_kernel, line, units), out_shape=(...  108 us
    pallas_call x1, Pallas kernels, reduced(): pl.pallas_call(functools.partial(reduce_kernel, line), out_shape=(jax.Sha...  62.4 us
    dot_general x1, matrix products, on_device(): jnp.dot(tokens[0], gate_up, preferred_element_type=jnp.float32)  14.7 us
    dot_general x1, matrix products, on_device(): lax.dot_general(jnp.concatenate([grad_gate, grad_up], axis=1), gate_up, c...  13.9 us
    dot_general x1, matrix products, on_device(): lax.dot_general(tokens[1], hidden, contract_tok, preferred_element_type=j...  9.96 us
    dot_general x1, matrix products, on_device(): jnp.dot(tokens[1], down_full, preferred_element_type=jnp.float32)  9.82 us

profile of v4, /device:TPU:0, one launch (start us, length us, event | category | flops | bytes accessed | tf_op | source)
XLA Modules:
  0.0 223.5 jit_solution(10615940661789775671)
XLA Ops:
  0.6 107.7 %gather_all.1 = (bf16[2048,1024]{1,0:T(8,128)(2,1)}, bf16[2048,512]{1,0:T(8,128)(2,1)}, bf16[2,2048,2048]{2,1,0:T(8,128)(2,1)}) custom-call(bf16[256,2048]{1,0:T(8,128)(2,1)} %gate_w.1, bf16[256,2048]{1,0:T(8,128)(2,1)} %up_w.1, bf16[256,2048]{1,0:T(8,128)(2,1)} %down_w.1, bf16[512,2048]{1,0:T(8,128)(2,1)} %toks.1, bf16[512,2048]{1,0:T(8,128)(2,1)} %cots.1), custom_call_target="tpu_custom_call" | custom-call | tf_op jit(solution)/shard_map/gather_all/pallas_call | solution.py:199
  108.3 0.0 copy-start.1
  108.3 14.7 %fusion = f32[2048,1024]{0,1:T(8,128)} fusion(bf16[2048,1024]{1,0:T(8,128)(2,1)} %get-tuple-element.9, bf16[2,2048,2048]{2,1,0:T(8,128)(2,1)} %get-tuple-element.7), kind=kOutput, calls=%fused_computation | convolution fusion | flops 8589934592 | bytes 20971520 | tf_op jit(solution)/shard_map/dot_general | solution.py:494
  123.0 0.0 copy-done.1
  123.0 0.0 copy-start.2
  123.0 10.0 %fusion.13.g_in = bf16[2048,512]{1,0:T(8,128)(2,1)} fusion(bf16[2,2048,2048]{2,1,0:T(8,128)(2,1)S(1)} %copy-done.1, f32[2048,1024]{0,1:T(8,128)} %fusion), kind=kOutput, calls=%fused_computation.18 | convolution fusion | flops 4302307328 | bytes 18874368 | tf_op jit(solution)/shard_map/dot_general | solution.py:507
  133.0 0.0 copy-done.2
  133.0 9.8 %multiply_convert_fusion.2 = (bf16[2048,512]{0,1:T(8,128)(2,1)}, bf16[2048,512]{0,1:T(8,128)(2,1)}) fusion(f32[2048,1024]{0,1:T(8,128)} %fusion, bf16[2048,512]{1,0:T(8,128)(2,1)S(1)} %copy-done.2, bf16[2,2048,2048]{2,1,0:T(8,128)(2,1)S(1)} %copy-done.1), kind=kOutput, calls=%fused_computation.15 | convolution fusion | flops 4308598784 | bytes 23068672 | tf_op jit(solution)/shard_map/dot_general | solution.py:496
  142.8 13.9 %convolution_convert_fusion.p_in = bf16[2048,2048]{1,0:T(8,128)(2,1)} fusion(bf16[2048,1024]{1,0:T(8,128)(2,1)} %get-tuple-element.9, bf16[2048,512]{0,1:T(8,128)(2,1)} %get-tuple-element.13, bf16[2048,512]{0,1:T(8,128)(2,1)} %get-tuple-element.12), kind=kOutput, calls=%fused_computation.7 | convolution fusion | flops 8602517504 | bytes 16777216 | tf_op jit(solution)/shard_map/dot_general | solution.py:510
  156.8 62.4 %reduce_all.1 = (bf16[512,2048]{1,0:T(8,128)(2,1)}, bf16[256,2048]{1,0:T(8,128)(2,1)}) custom-call(bf16[2048,2048]{1,0:T(8,128)(2,1)} %convolution_convert_fusion.p_in, bf16[2048,512]{1,0:T(8,128)(2,1)} %fusion.13.g_in), custom_call_target="tpu_custom_call" | custom-call | tf_op jit(solution)/shard_map/reduce_all/pallas_call | solution.py:456
  219.2 0.0 copy-start
  219.2 2.9 %convert_multiply_fusion = f32[256,2048]{1,0:T(8,128)} fusion(bf16[256,2048]{1,0:T(8,128)(2,1)} %get-tuple-element.11), kind=kLoop, calls=%fused_computation.19 | loop fusion | flops 1048576 | bytes 3145728 | tf_op jit(solution)/shard_map/mul | solution.py:518
  222.2 0.0 copy-done
  222.2 1.3 copy.8
Async XLA Ops:
  108.3 14.7 %copy-start.1 = (bf16[2,2048,2048]{2,1,0:T(8,128)(2,1)S(1)}, bf16[2,2048,2048]{2,1,0:T(8,128)(2,1)}, u32[]{:S(2)}) copy-start(bf16[2,2048,2048]{2,1,0:T(8,128)(2,1)} %get-tuple-element.7) | copy-start | bytes 50331652
  123.0 10.0 %copy-start.2 = (bf16[2048,512]{1,0:T(8,128)(2,1)S(1)}, bf16[2048,512]{1,0:T(8,128)(2,1)}, u32[]{:S(2)}) copy-start(bf16[2048,512]{1,0:T(8,128)(2,1)} %get-tuple-element.8) | copy-start | bytes 6291460
  219.2 3.0 %copy-start = (bf16[512,2048]{1,0:T(8,128)(2,1)S(1)}, bf16[512,2048]{1,0:T(8,128)(2,1)}, u32[]{:S(2)}) copy-start(bf16[512,2048]{1,0:T(8,128)(2,1)} %get-tuple-element.16) | copy-start | bytes 6291460
